TPU v7x, 512 devices: a whole 4x8x8 slice. The times are simulated.
512 devices in a mesh: ep: 32 (over z, x), tp: 16 (over y, core).
Axes of the slice: x: 4, y: 8, z: 8, core: 2. Of those that a mesh axis runs over, the one named last changes fastest.
Arguments:
- mixer_input: bfloat16 [4096, 2048], P('ep'), may hold values from -6 to 6
- mixer_gain: float32 [2048], replicated, may hold values from 0.1 to 1.9
- outer_weight: bfloat16 [2048, 1024], P(None, 'tp'), may hold values from -0.125 to 0.125
- inner_weight: bfloat16 [2048, 1024], P(None, 'tp'), may hold values from -0.125 to 0.125
- value_weight: bfloat16 [2048, 1024], P(None, 'tp'), may hold values from -0.125 to 0.125
- conv_kernel: bfloat16 [3, 1024], P(None, 'tp'), may hold values from -3 to 3
- group_gain: float32 [1024], P('tp'), may hold values from 0.1 to 1.9
- mixer_out_weight: bfloat16 [1024, 2048], P(None, 'tp'), may hold values from -0.1875 to 0.1875
- expert_input: bfloat16 [8192, 2048], P('ep'), may hold values from -6 to 6
- expert_gain: float32 [2048], replicated, may hold values from 0.1 to 1.9
- routes: int32 [8192, 2], P('ep'), may hold values from 0 to 31, all different within a row; in each aligned block of 256 rows (0 to 255, 256 to 511, ...) at most 32 rows name the same one
- route_weight: float32 [8192, 2], P('ep'), may hold values from 0.1 to 1
- expert_gate: bfloat16 [32, 2048, 3584], P('ep', None, 'tp'), may hold values from -0.125 to 0.125
- expert_up: bfloat16 [32, 2048, 3584], P('ep', None, 'tp'), may hold values from -0.125 to 0.125
- expert_down: bfloat16 [32, 3584, 2048], P('ep', None, 'tp'), may hold values from -0.09375 to 0.09375
Outputs:
- mixed_tokens: bfloat16 [4096, 2048], P('ep', 'tp')
- expert_tokens: bfloat16 [8192, 2048], P('ep', 'tp')
Inputs may be any that keep to these rules, and one draw needn't show every extreme that they name: `routes`: each row names 2 different experts. Within the rows of one index of ep no expert is named by more than 32 rows, a bound that some block reaches of them.
All inputs are finite; a program needn't handle non-finite values.
Results may differ from a plain program's by a relative error of at most 0.014.
Values may be sent and summed in bfloat16 or wider, within the bound.
A program may use at most 64 MiB of HBM per device.

v0:
```python
import jax
import jax.numpy as jnp
from jax import lax
from jax.sharding import PartitionSpec as P

GROUP = 64


EPS = 1e-06


def from_behind(block, axis, distance):
    devices = range(lax.axis_size(axis))
    route = [(i - distance, i) for i in devices if i - distance in devices]
    return lax.ppermute(block, axis, route)


def laid_out(tiles, dim):
    tiles = jnp.moveaxis(tiles, 0, dim)
    lengths = tiles.shape
    return tiles.reshape(*lengths[:dim], lengths[dim] * lengths[dim + 1], *lengths[dim + 2 :])


def sent_to_all(value, axis):
    size = lax.axis_size(axis)
    return lax.all_to_all(
        jnp.broadcast_to(value[None], (size, *value.shape)), axis, 0, 0, tiled=True
    )


def collect(value, axis, dim):
    return laid_out(sent_to_all(value, axis), dim)


def rms_scale(values, gain):
    floats = values.astype(jnp.float32)
    scale = lax.rsqrt(jnp.mean(floats * floats, axis=-1, keepdims=True) + EPS)
    return floats * scale * gain


def per_device(
    mixer_input,
    mixer_gain,
    outer_weight,
    inner_weight,
    value_weight,
    conv_kernel,
    group_gain,
    mixer_out_weight,
    expert_input,
    expert_gain,
    routes,
    route_weight,
    expert_gate,
    expert_up,
    expert_down,
):
    mix_count = mixer_input.shape[0]
    normed_a = rms_scale(mixer_input, mixer_gain).astype(jnp.bfloat16)
    outer = jnp.dot(normed_a, outer_weight, preferred_element_type=jnp.float32).astype(jnp.bfloat16)
    inner = jnp.dot(normed_a, inner_weight, preferred_element_type=jnp.float32).astype(jnp.bfloat16)
    values = jnp.dot(normed_a, value_weight, preferred_element_type=jnp.float32).astype(
        jnp.bfloat16
    )
    product = inner.astype(jnp.float32) * values.astype(jnp.float32)
    earlier_rows = from_behind(product[mix_count - 2 :], "ep", 1)
    padded = jnp.concatenate([earlier_rows, product], axis=0)
    kernel = conv_kernel.astype(jnp.float32)
    conv_sum = (
        kernel[0] * padded[0:mix_count]
        + kernel[1] * padded[1 : mix_count + 1]
        + kernel[2] * padded[2 : mix_count + 2]
    )
    gated = outer.astype(jnp.float32) * conv_sum
    grouped = gated.reshape(mix_count, -1, GROUP)
    grouped = rms_scale(grouped, group_gain.reshape(-1, GROUP))
    grouped = grouped.reshape(mix_count, -1).astype(jnp.bfloat16)
    weight_rows = mixer_out_weight
    mixed_tokens = jnp.dot(
        collect(grouped, "tp", 1), weight_rows, preferred_element_type=jnp.float32
    ).astype(jnp.bfloat16)
    exp_count, picks_each = routes.shape
    width = expert_input.shape[1]
    experts = expert_gate.shape[0] * lax.axis_size("ep")
    capacity = 2 * picks_each * exp_count // experts
    normed_b = rms_scale(expert_input, expert_gain).astype(jnp.bfloat16)
    picks = routes.reshape(-1)
    onehot = (picks[:, None] == jnp.arange(experts, dtype=jnp.int32)[None, :]).astype(jnp.int32)
    rank = jnp.sum((jnp.cumsum(onehot, axis=0) - onehot) * onehot, axis=1)
    slot = picks * capacity + rank
    token = jnp.arange(exp_count * picks_each, dtype=jnp.int32) // picks_each
    table = jnp.zeros((experts * capacity,), jnp.int32).at[slot].set(token + 1)
    valid = table > 0
    gathered_rows = jnp.take(normed_b, jnp.maximum(table - 1, 0), axis=0)
    buffer = jnp.where(valid[:, None], gathered_rows, 0).reshape(experts, capacity, width)
    gate_weight = expert_gate[0]
    up_weight = expert_up[0]
    down_weight = expert_down[0]
    out_cols = down_weight.shape[1]
    span = width // lax.axis_size("tp")
    outgoing = lax.dynamic_slice_in_dim(buffer, lax.axis_index("tp") * span, span, 2)
    received = lax.all_to_all(outgoing, "ep", split_axis=0, concat_axis=0, tiled=True)
    sources = received.shape[0]
    count = received.shape[1]
    piece = lax.all_gather(received, "tp", axis=2, tiled=True)
    span = piece.shape[2]
    flat_piece = piece.reshape(sources * count, span)
    gate = jnp.dot(flat_piece, gate_weight, preferred_element_type=jnp.float32)
    up_value = jnp.dot(flat_piece, up_weight, preferred_element_type=jnp.float32)
    hidden = (jax.nn.silu(gate) * up_value).astype(jnp.bfloat16)
    weight_rows = down_weight
    results = jnp.dot(
        lax.all_gather(hidden, "tp", axis=1, tiled=True),
        weight_rows,
        preferred_element_type=jnp.float32,
    ).astype(jnp.bfloat16)
    returned = lax.all_to_all(
        results.reshape(sources, count, out_cols), "ep", split_axis=0, concat_axis=0, tiled=True
    )
    flat_returned = returned.reshape(experts * capacity, out_cols)
    chosen = (
        jnp.take(flat_returned, slot, axis=0)
        .astype(jnp.float32)
        .reshape(exp_count, picks_each, out_cols)
    )
    weighted = jnp.sum(chosen * route_weight[..., None], axis=1)
    expert_tokens = weighted.astype(jnp.bfloat16)
    return (mixed_tokens, expert_tokens)


def solution(mesh):
    placed = (
        P("ep", None),
        P(),
        P(None, "tp"),
        P(None, "tp"),
        P(None, "tp"),
        P(None, "tp"),
        P("tp"),
        P(None, "tp"),
        P("ep", None),
        P(),
        P("ep", None),
        P("ep", None),
        P("ep", None, "tp"),
        P("ep", None, "tp"),
        P("ep", None, "tp"),
    )
    return jax.shard_map(
        per_device,
        mesh=mesh,
        in_specs=placed,
        out_specs=(P("ep", "tp"), P("ep", "tp")),
        check_vma=False,
    )
```

profile of v0, /device:TPU:1, one launch (start us, length us, event | category | flops | bytes accessed | tf_op | source)
XLA Modules:
  0.0 200.1 jit_solution(5589004506806771158)
XLA Ops:
  7.2 0.9 copy.25
  8.1 0.1 eq.26
  8.4 0.7 broadcast_multiply_fusion
  9.1 1.2 reduce-window.6
  10.3 0.2 slice_reduce_fusion
  10.5 0.1 copy.30
  10.7 0.1 mul.160
  11.0 2.4 %scatter_custom_fusion = s32[1024]{0:T(1024)S(1)} fusion(s32[512]{0:T(512)S(1)} %bitcast.57, s32[512]{0:T(512)S(1)} %fusion.28, s32[]{:T(128)} %constant.74.clone.1), kind=kCustom, calls=%fused_computation.67 | custom fusion | bytes 4100 | tf_op jit(solution)/shard_map/scatter | solution.py:92
  13.6 1.5 fusion
  15.1 1.5 fusion.2
  16.7 6.0 %gather_fusion = bf16[1024,2048]{1,0:T(8,128)(2,1)} fusion(bf16[256,2048]{1,0:T(8,128)(2,1)S(1)} %fusion.2, s32[1024]{0:T(1024)S(1)} %fusion.26), kind=kCustom, calls=%fused_computation | custom fusion | bytes 8392704 | tf_op jit(solution)/shard_map/jit(_take)/gather | solution.py:94
  22.6 1.4 fusion.15
  24.0 24.9 %all_to_all.15 = bf16[32,32,128]{2,1,0:T(8,128)(2,1)} all-to-all(bf16[32,32,128]{2,1,0:T(8,128)(2,1)S(1)} %fusion.15), channel_id=1, replica_groups=mesh['ep'=32,'tp'=16] {'ep'}, dimensions={0} | all-to-all | bytes 524288 | tf_op jit(solution)/shard_map/all_to_all | solution.py:102
  49.0 50.3 %all-gather.3.cloned.1.call-done = bf16[32,32,2048]{2,1,0:T(8,128)(2,1)} async-done(((bf16[32,32,128]{2,1,0:T(8,128)(2,1)}), bf16[32,32,2048]{2,1,0:T(8,128)(2,1)}) %all-gather.3.cloned.1.call-update) | async-done | bytes 4194320 | tf_op jit(solution)/shard_map/all_gather | solution.py:105
  99.3 3.7 %fusion.13 = f32[1024,224]{0,1:T(8,128)S(1)} fusion(bf16[1024,2048]{1,0:T(8,128)(2,1)} %bitcast.59, bf16[1,2048,224]{1,2,0:T(8,128)(2,1)S(1)} %copy-done), kind=kOutput, calls=%fused_computation.26 | convolution fusion | flops 939524096 | bytes 6029312 | tf_op jit(solution)/shard_map/dot_general | solution.py:108
  103.1 2.3 %fusion.3 = bf16[1024,224]{0,1:T(8,128)(2,1)} fusion(bf16[1024,2048]{1,0:T(8,128)(2,1)S(1)} %bitcast.60, bf16[1,2048,224]{1,2,0:T(8,128)(2,1)S(1)} %copy-done.8, f32[1024,224]{0,1:T(8,128)S(1)} %fusion.13), kind=kOutput, calls=%fused_computation.11 | convolution fusion | flops 940900352 | bytes 6488064 | tf_op jit(solution)/shard_map/dot_general | solution.py:109
  105.4 0.2 fusion.8
  105.6 0.4 fusion.6
  106.0 0.4 fusion.5
  106.5 2.1 %collective-permute-start = (f32[2,64]{0,1:T(8,128)S(1)}, f32[2,64]{0,1:T(8,128)S(1)}, u32[]{:S(2)}, u32[]{:S(2)}) collective-permute-start(f32[2,64]{0,1:T(8,128)S(1)} %slice.36), channel_id=1, source_target_pairs={{0,16},{16,32},{32,48},{48,64},{64,80},{80,96},{96,112},{112,128},... | collective-permute-start | bytes 1544 | tf_op jit(solution)/shard_map/ppermute | solution.py:15
  108.9 0.8 collective-permute-done
  109.6 0.4 multiply_reduce_fusion.1
  110.1 0.8 broadcast_in_dim.53
  110.9 5.4 %all-to-all-start = ((bf16[16,128,64]{1,2,0:T(8,128)(2,1)}), bf16[16,128,64]{1,2,0:T(8,128)(2,1)S(1)}, u32[]{:S(2)}, u32[]{:S(2)}) async-start(bf16[16,128,64]{1,2,0:T(8,128)(2,1)} %broadcast_in_dim.53), calls=%async_computation | async-start | bytes 524288 | tf_op jit(solution)/shard_map/all_to_all | solution.py:26
  116.3 45.8 %all-gather.5.cloned.1.call-done = bf16[1024,3584]{0,1:T(8,128)(2,1)} async-done(((bf16[1024,224]{0,1:T(8,128)(2,1)}), bf16[1024,3584]{0,1:T(8,128)(2,1)}) %all-gather.5.cloned.1.call-update) | async-done | bytes 7340048 | tf_op jit(solution)/shard_map/all_gather | solution.py:113
  162.1 5.9 %convolution_convert_fusion = bf16[1024,128]{1,0:T(8,128)(2,1)} fusion(bf16[1024,3584]{0,1:T(8,128)(2,1)} %all-gather.5.cloned.1.call-done, bf16[1,3584,128]{2,1,0:T(8,128)(2,1)S(1)} %copy-done.9), kind=kOutput, calls=%fused_computation.12 | convolution fusion | flops 939655168 | bytes 8519680 | tf_op jit(solution)/shard_map/dot_general | solution.py:112
  168.0 10.1 %all-to-all-start.2 = ((bf16[32,32,128]{2,1,0:T(8,128)(2,1)}), bf16[32,32,128]{2,1,0:T(8,128)(2,1)S(1)}, u32[]{:S(2)}, u32[]{:S(2)}) async-start(bf16[32,32,128]{2,1,0:T(8,128)(2,1)} %bitcast.13), calls=%async_computation.2 | async-start | bytes 524288 | tf_op jit(solution)/shard_map/all_to_all | solution.py:117
  178.2 0.2 copy.29
  178.5 0.9 convolution_convert_fusion.1
  179.4 10.4 %all-to-all-done.2 = bf16[32,32,128]{2,1,0:T(8,128)(2,1)S(1)} async-done(((bf16[32,32,128]{2,1,0:T(8,128)(2,1)}), bf16[32,32,128]{2,1,0:T(8,128)(2,1)S(1)}, u32[]{:S(2)}, u32[]{:S(2)}) %all-to-all-start.2) | async-done | bytes 262176 | tf_op jit(solution)/shard_map/all_to_all | solution.py:117
  189.8 1.3 gather_fusion.1
  191.2 2.1 %multiply_reduce_fusion = bf16[256,128]{1,0:T(8,128)(2,1)} fusion(bf16[256,2,128]{2,1,0:T(2,128)(2,1)S(1)} %bitcast.55, pred[256,2]{1,0:T(8,128)(4,1)S(1)} %copy.29, f32[256,2]{1,0:T(8,128)S(1)} %copy.31), kind=kLoop, calls=%fused_computation.30 | loop fusion | flops 229376 | bytes 199168 | tf_op jit(solution)/shard_map/reduce_sum | solution.py:126
  (56 shorter events, 1.2 us)
Async XLA Ops:
  7.2 92.1 %copy-start = (bf16[1,2048,224]{1,2,0:T(8,128)(2,1)S(1)}, bf16[1,2048,224]{1,2,0:T(8,128)(2,1)}, u32[]{:S(2)}) copy-start(bf16[1,2048,224]{1,2,0:T(8,128)(2,1)} %param.27) | copy-start | bytes 2752516
  7.2 92.1 %all-gather.3.cloned.1.call-start = ((), (), s32[]{:S(2)}) async-start(), calls=%async_computation.3 | async-start | bytes 4456448 | tf_op jit(solution)/shard_map/all_gather | solution.py:105
  22.6 80.4 %copy-start.8 = (bf16[1,2048,224]{1,2,0:T(8,128)(2,1)S(1)}, bf16[1,2048,224]{1,2,0:T(8,128)(2,1)}, u32[]{:S(2)}) copy-start(bf16[1,2048,224]{1,2,0:T(8,128)(2,1)} %param.28) | copy-start | bytes 2752516
  49.0 113.1 %all-gather.5.cloned.1.call-start = ((), (), s32[]{:S(2)}) async-start(), calls=%async_computation.4 | async-start | bytes 7798784 | tf_op jit(solution)/shard_map/all_gather | solution.py:113
  99.3 3.8 %copy-start.7 = (bf16[32,32,2048]{2,1,0:T(8,128)(2,1)S(1)}, bf16[32,32,2048]{2,1,0:T(8,128)(2,1)}, u32[]{:S(2)}) copy-start(bf16[32,32,2048]{2,1,0:T(8,128)(2,1)} %all-gather.3.cloned.1.call-done) | copy-start | bytes 12582916
  103.0 2.4 %copy-start.1 = (bf16[128,2048]{1,0:T(8,128)(2,1)S(1)}, bf16[128,2048]{1,0:T(8,128)(2,1)}, u32[]{:S(2)}) copy-start(bf16[128,2048]{1,0:T(8,128)(2,1)} %param.15) | copy-start | bytes 1572868
  103.1 2.6 %copy-start.10 = (bf16[2048,64]{0,1:T(8,128)(2,1)S(1)}, bf16[2048,64]{0,1:T(8,128)(2,1)}, u32[]{:S(2)}) copy-start(bf16[2048,64]{0,1:T(8,128)(2,1)} %param.18) | copy-start | bytes 786436
  103.1 2.6 %copy-start.13 = (f32[2048]{0:T(1024)S(1)}, f32[2048]{0:T(1024)}, u32[]{:S(2)}) copy-start(f32[2048]{0:T(1024)} %param.16) | copy-start | bytes 24580
  103.1 2.9 %copy-start.11 = (bf16[2048,64]{0,1:T(8,128)(2,1)S(1)}, bf16[2048,64]{0,1:T(8,128)(2,1)}, u32[]{:S(2)}) copy-start(bf16[2048,64]{0,1:T(8,128)(2,1)} %param.19) | copy-start | bytes 786436
  103.1 5.5 %copy-start.5 = (bf16[3,64]{1,0:T(4,128)(2,1)S(1)}, bf16[3,64]{1,0:T(4,128)(2,1)}, u32[]{:S(2)}) copy-start(bf16[3,64]{1,0:T(4,128)(2,1)} %param.20) | copy-start | bytes 1156
  103.1 6.5 %copy-start.12 = (bf16[2048,64]{0,1:T(8,128)(2,1)S(1)}, bf16[2048,64]{0,1:T(8,128)(2,1)}, u32[]{:S(2)}) copy-start(bf16[2048,64]{0,1:T(8,128)(2,1)} %param.17) | copy-start | bytes 786436
  105.4 4.6 %copy-start.6 = (f32[64]{0:T(128)S(1)}, f32[64]{0:T(128)}, u32[]{:S(2)}) copy-start(f32[64]{0:T(128)} %param.21) | copy-start | bytes 772
  105.4 56.7 %copy-start.9 = (bf16[1,3584,128]{2,1,0:T(8,128)(2,1)S(1)}, bf16[1,3584,128]{2,1,0:T(8,128)(2,1)}, u32[]{:S(2)}) copy-start(bf16[1,3584,128]{2,1,0:T(8,128)(2,1)} %param.29) | copy-start | bytes 2752516
  106.5 3.2 %collective-permute-start = (f32[2,64]{0,1:T(8,128)S(1)}, f32[2,64]{0,1:T(8,128)S(1)}, u32[]{:S(2)}, u32[]{:S(2)}) collective-permute-start(f32[2,64]{0,1:T(8,128)S(1)} %slice.36), channel_id=1, source_target_pairs={{0,16},{16,32},{32,48},{48,64},{64,80},{80,96},{96,112},{112,128},... | collective-permute-start | bytes 1544 | tf_op jit(solution)/shard_map/ppermute | solution.py:15
  110.9 57.2 %all-to-all-start = ((bf16[16,128,64]{1,2,0:T(8,128)(2,1)}), bf16[16,128,64]{1,2,0:T(8,128)(2,1)S(1)}, u32[]{:S(2)}, u32[]{:S(2)}) async-start(bf16[16,128,64]{1,2,0:T(8,128)(2,1)} %broadcast_in_dim.53), calls=%async_computation | async-start | bytes 524288 | tf_op jit(solution)/shard_map/all_to_all | solution.py:26
  116.3 61.9 %copy-start.3 = (s32[256,2]{0,1:T(2,128)S(1)}, s32[256,2]{0,1:T(2,128)}, u32[]{:S(2)}) copy-start(s32[256,2]{0,1:T(2,128)} %param.25) | copy-start | bytes 6148
  116.3 62.1 %copy-start.4 = (f32[256,2]{0,1:T(2,128)S(1)}, f32[256,2]{0,1:T(2,128)}, u32[]{:S(2)}) copy-start(f32[256,2]{0,1:T(2,128)} %param.26) | copy-start | bytes 6148
  116.3 62.2 %copy-start.2 = (bf16[1024,128]{1,0:T(8,128)(2,1)S(1)}, bf16[1024,128]{1,0:T(8,128)(2,1)}, u32[]{:S(2)}) copy-start(bf16[1024,128]{1,0:T(8,128)(2,1)} %param.22) | copy-start | bytes 786436
  168.0 21.8 %all-to-all-start.2 = ((bf16[32,32,128]{2,1,0:T(8,128)(2,1)}), bf16[32,32,128]{2,1,0:T(8,128)(2,1)S(1)}, u32[]{:S(2)}, u32[]{:S(2)}) async-start(bf16[32,32,128]{2,1,0:T(8,128)(2,1)} %bitcast.13), calls=%async_computation.2 | async-start | bytes 524288 | tf_op jit(solution)/shard_map/all_to_all | solution.py:117
Sparse Core Ops, SparseCore 0:
  49.1 50.1 all-gather.2
  105.5 56.5 all-gather.4
where the time goes:
time: 201 us; the launch traced here: 200 us
  waiting for transfers between devices  107 us (53%)
  blocking collectives  24.9 us (12%)
  starting transfers between devices  17.8 us (9%)
  between operations  14.4 us (7%)
  matrix products  13.9 us (7%)
  local copies, waits for them, and re-layouts  13 us (6%)
  other arithmetic  8.83 us (4%)
    all_gather x1, waiting for transfers between devices, per_device(): piece = lax.all_gather(received, 'tp', axis=2, tiled=True)  50.3 us
    all_gather x1, waiting for transfers between devices, per_device(): lax.all_gather(hidden, 'tp', axis=1, tiled=True)  45.8 us
    all_to_all x1, blocking collectives, per_device(): lax.all_to_all(outgoing, 'ep', split_axis=0, concat_axis=0, tiled=True)  24.9 us
    all_to_all x1, waiting for transfers between devices, per_device(): lax.all_to_all(results.reshape(sources, count, out_cols), 'ep', split_axi...  10.4 us
    all_to_all x1, starting transfers between devices, per_device(): lax.all_to_all(results.reshape(sources, count, out_cols), 'ep', split_axi...  10.1 us
    gather x1, local copies, waits for them, and re-layouts, per_device(): gathered_rows = jnp.take(normed_b, jnp.maximum(table - 1, 0), axis=0)  5.98 us
    dot_general x1, matrix products, per_device(): jnp.dot(lax.all_gather(hidden, 'tp', axis=1, tiled=True), weight_rows, pr...  5.91 us
    all_to_all x1, starting transfers between devices, sent_to_all(): lax.all_to_all(jnp.broadcast_to(value[None], (size, *value.shape)), axis,...  5.42 us
  transfers between devices with their start and end apart: 5, of which 4 were waited for; matrix products, arithmetic and copies ran while one was open for 5% of the time, Pallas kernels for 0%

commit v1 on v0

v1 whole, which is shorter than its diff:
```python
import functools

import jax
import jax.numpy as jnp
from jax import lax
from jax.experimental import pallas as pl
from jax.experimental.pallas import tpu as pltpu
from jax.sharding import PartitionSpec as P

EPS = 1e-06
MESH = pl.DeviceIdType.MESH
F32 = jnp.float32
BF16 = jnp.bfloat16
NZ, NX = 8, 4
N_EP = NZ * NX
N_Y = 8
N_TP = 2 * N_Y
BATCHES = 4
CAP = 32
PER = N_EP // BATCHES


def hops(n, d):
    return min(d, n - d)


def offset_order():
    pairs = [(dz, dx) for dz in range(NZ) for dx in range(NX)]
    return sorted(pairs, key=lambda o: (hops(NZ, o[0]) + hops(NX, o[1]), hops(NZ, o[0]), o))


OFFSETS = offset_order()
GROUPS = [OFFSETS[8:16], OFFSETS[16:24], OFFSETS[24:32], OFFSETS[0:8]]


def nt(a, b):
    return lax.dot_general(a, b, (((1,), (1,)), ((), ())), preferred_element_type=F32)


def nn(a, b):
    return lax.dot_general(a, b, (((1,), (0,)), ((), ())), preferred_element_type=F32)


def eye(n):
    return (
        lax.broadcasted_iota(jnp.int32, (n, n), 0) == lax.broadcasted_iota(jnp.int32, (n, n), 1)
    )


def column(row, mask):
    return jnp.sum(jnp.where(mask, row, 0.0), axis=1, keepdims=True)


def kernel(
    mixin_h, mgain_h, outer_h, inner_h, value_h, conv_h, ggain_h, mout_h,
    expin_h, egain_h, routes_h, rweight_h, gate_h, up_h, down_h,
    mixed_o, tokens_o,
    mixin, mgain, mproj, conv, ggain, mout,
    expin, egain, routes, rweight, gateup, down,
    onehot, pos32, wsel32, combine, wide_t, send_b, xs, hs, y_b, ret,
    down_t, mout_t, grouped, prod_s, halo, outer_s,
    load_sem, disp_s, disp_r, ret_s, ret_r, ring_s, ring_r, part_s, part_r, halo_sem,
):
    ep = lax.axis_index("ep")
    tp = lax.axis_index("tp")
    z, x = ep // NX, lax.rem(ep, NX)
    core = lax.rem(tp, 2)
    mate = tp + 1 - 2 * core
    y_of = tp // 2

    def ep_at(dz, dx):
        return lax.rem(z + dz + NZ, NZ) * NX + lax.rem(x + dx + NX, NX)

    def ring_tp(d):
        return lax.rem(tp + 2 * d + N_TP, N_TP)

    loads = {}
    for i, (name, src, dst) in enumerate(
        [
            ("routes", routes_h, routes),
            ("expin", expin_h, expin),
            ("egain", egain_h, egain),
            ("mixin", mixin_h, mixin),
            ("mgain", mgain_h, mgain),
            ("outer", outer_h, mproj.at[pl.ds(0, 64)]),
            ("inner", inner_h, mproj.at[pl.ds(64, 64)]),
            ("value", value_h, mproj.at[pl.ds(128, 64)]),
            ("conv", conv_h, conv),
            ("ggain", ggain_h, ggain),
            ("rweight", rweight_h, rweight),
            ("gate", gate_h, gateup.at[pl.ds(0, 224)]),
            ("up", up_h, gateup.at[pl.ds(224, 224)]),
            ("down", down_h, down),
            ("mout", mout_h, mout),
        ]
    ):
        loads[name] = pltpu.make_async_copy(src, dst, load_sem.at[i])
        loads[name].start()

    barrier = pltpu.get_barrier_semaphore()
    for dz, dx in OFFSETS[1:]:
        pl.semaphore_signal(barrier, inc=1, device_id=(ep_at(dz, dx), tp), device_id_type=MESH)
    for other in (ring_tp(1), ring_tp(-1), mate):
        pl.semaphore_signal(barrier, inc=1, device_id=(ep, other), device_id_type=MESH)

    loads["routes"].wait()
    first, second = routes[0:1, :], routes[1:2, :]
    expert = lax.broadcasted_iota(jnp.int32, (N_EP, 256), 0)
    is_first = first == expert
    named = is_first | (second == expert)
    before = lax.broadcasted_iota(jnp.int32, (256, 256), 0) < lax.broadcasted_iota(
        jnp.int32, (256, 256), 1
    )
    rank = nn(jnp.where(named, 1.0, 0.0).astype(BF16), jnp.where(before, 1.0, 0.0).astype(BF16))
    pos32[...] = jnp.where(named, rank, -1.0)
    slot = lax.broadcasted_iota(jnp.int32, (CAP, 256), 0).astype(F32)
    for e in range(N_EP):
        onehot[e * CAP : (e + 1) * CAP, :] = jnp.where(slot == pos32[e : e + 1, :], 1.0, 0.0).astype(
            BF16
        )

    loads["expin"].wait()
    loads["egain"].wait()
    own_features = pl.ds(pl.multiple_of(tp * 128, 128), 128)
    rows = expin[...].astype(F32)
    scale = lax.rsqrt(jnp.mean(rows * rows, axis=-1, keepdims=True) + EPS)
    normed_b = (expin[:, own_features].astype(F32) * scale * egain[:, own_features]).astype(BF16)
    send_b[...] = nn(onehot[...], normed_b).astype(BF16)

    pl.semaphore_wait(barrier, N_EP - 1 + 3)

    def dispatch(b, i):
        dz, dx = GROUPS[b][i]
        target = ep_at(-dz, -dx)
        return pltpu.make_async_remote_copy(
            src_ref=send_b.at[pl.ds(pl.multiple_of(target * CAP, CAP), CAP)],
            dst_ref=xs.at[b, pl.ds(i * CAP, CAP), own_features],
            send_sem=disp_s.at[b, i],
            recv_sem=disp_r.at[b, i],
            device_id=(target, tp),
            device_id_type=MESH,
        )

    for b in range(BATCHES):
        for i, o in enumerate(GROUPS[b]):
            if o != (0, 0):
                dispatch(b, i).start()
            else:
                xs[b, i * CAP : (i + 1) * CAP, own_features] = send_b[
                    pl.ds(pl.multiple_of(ep * CAP, CAP), CAP), :
                ]

    for name in ("mixin", "mgain", "outer", "inner", "value"):
        loads[name].wait()
    rows_a = mixin[...].astype(F32)
    scale_a = lax.rsqrt(jnp.mean(rows_a * rows_a, axis=-1, keepdims=True) + EPS)
    normed_a = (rows_a * scale_a * mgain[...]).astype(BF16)
    projected = nt(mproj[...], normed_a).astype(BF16).astype(F32)
    outer_s[...] = projected[0:64]
    prod_s[...] = projected[64:128] * projected[128:192]
    next_ep = lax.rem(ep + 1, N_EP)
    halo_copy = pltpu.make_async_remote_copy(
        src_ref=prod_s,
        dst_ref=halo,
        send_sem=halo_sem.at[0],
        recv_sem=halo_sem.at[1],
        device_id=(next_ep, tp),
        device_id_type=MESH,
    )
    halo_copy.start()

    def mixer_group():
        halo_copy.wait()
        for name in ("conv", "ggain"):
            loads[name].wait()
        product = prod_s[...]
        behind = jnp.where(ep > 0, halo[...], 0.0)
        lane = lax.broadcasted_iota(jnp.int32, (64, 128), 1)
        one = jnp.where(lane < 1, pltpu.roll(behind, 1, 1), pltpu.roll(product, 1, 1))
        two = jnp.where(lane < 2, pltpu.roll(behind, 2, 1), pltpu.roll(product, 2, 1))
        mask = eye(64)
        taps = [column(conv[i : i + 1, :].astype(F32), mask) for i in range(3)]
        conv_sum = taps[0] * two + taps[1] * one + taps[2] * product
        gated = outer_s[...] * conv_sum
        norm = lax.rsqrt(jnp.mean(gated * gated, axis=0, keepdims=True) + EPS)
        own = pl.ds(pl.multiple_of(tp * 64, 64), 64)
        grouped[own, :] = (gated * norm * column(ggain[...], mask)).astype(BF16)

    def prepare_combine():
        loads["rweight"].wait()
        weight = jnp.where(is_first, rweight[0:1, :], rweight[1:2, :])
        high = weight.astype(BF16).astype(F32)
        identity = jnp.where(eye(256), 1.0, 0.0).astype(BF16)
        for part, value in enumerate((high, weight - high)):
            wsel32[...] = value
            for e in range(N_EP):
                wide_t[e * CAP : (e + 1) * CAP, :] = jnp.where(
                    slot == pos32[e : e + 1, :], wsel32[e : e + 1, :], 0.0
                ).astype(BF16)
            combine[part] = nt(identity, wide_t[...]).astype(BF16)

    def prepare_down():
        loads["down"].wait()
        identity = jnp.where(eye(128), 1.0, 0.0).astype(BF16)
        down_t[...] = nt(identity, down[...]).astype(BF16)
        loads["mout"].wait()
        mout_t[...] = nt(identity, mout[...]).astype(BF16)

    def piece_of(kind, b):
        if kind == "x":
            return lambda j: xs.at[b, :, pl.ds(pl.multiple_of(j * 128, 128), 128)]
        if kind == "h":
            return lambda j: hs.at[b, pl.ds(pl.multiple_of(j * 224, 224), 224)]
        return lambda j: grouped.at[pl.ds(pl.multiple_of(j * 64, 64), 64)]

    started = []

    def send(src, dst, send_sem, recv_sem, to):
        copy = pltpu.make_async_remote_copy(
            src_ref=src, dst_ref=dst, send_sem=send_sem, recv_sem=recv_sem,
            device_id=(ep, to), device_id_type=MESH,
        )
        copy.start()
        started.append(copy)

    class Gather:
        def __init__(self, number, kind, b, far):
            self.n, self.piece = number, piece_of(kind, b)
            self.reach = {1: 4 if far > 0 else 3, -1: 4 if far < 0 else 3}

        def index(self, way, k):
            return k - 1 if way == 1 else self.reach[1] + k - 1

        def on_ring(self, ref, way, k):
            i = self.index(way, k)
            send(ref, ref, ring_s.at[self.n, i], ring_r.at[self.n, i], ring_tp(way))

        def to_mate(self, ref, i):
            send(ref, ref, part_s.at[self.n, i], part_r.at[self.n, i], mate)

        def wait(self, ref, sem):
            pltpu.make_async_remote_copy(
                src_ref=ref, dst_ref=ref, send_sem=part_s.at[self.n, 0], recv_sem=sem,
                device_id=(ep, mate), device_id_type=MESH,
            ).wait_recv()

        def first(self):
            ref = self.piece(tp)
            self.on_ring(ref, 1, 1)
            self.on_ring(ref, -1, 1)
            self.to_mate(ref, 7)

        def step(self, k):
            for way in (1, -1):
                if k > self.reach[way]:
                    continue
                ref = self.piece(ring_tp(-way * k))
                i = self.index(way, k)
                self.wait(ref, ring_r.at[self.n, i])
                if k < self.reach[way]:
                    self.on_ring(ref, way, k + 1)
                self.to_mate(ref, i)

        def finish(self):
            self.wait(self.piece(mate), part_r.at[self.n, 7])
            for way in (1, -1):
                for k in range(1, self.reach[way] + 1):
                    j = lax.rem(mate - 2 * way * k + N_TP, N_TP)
                    self.wait(self.piece(j), part_r.at[self.n, self.index(way, k)])

    def wait_dispatched(b):
        for i, o in enumerate(GROUPS[b]):
            if o != (0, 0):
                dispatch(b, i).wait_recv()

    def hidden(b):
        both = nt(gateup[...], xs[b])
        gate, up = both[0:224], both[224:448]
        own = pl.ds(pl.multiple_of(tp * 224, 224), 224)
        hs[b, own, :] = (gate / (1.0 + jnp.exp(-gate)) * up).astype(BF16)

    def give_back(b, i):
        dz, dx = GROUPS[b][i]
        target = ep_at(dz, dx)
        return pltpu.make_async_remote_copy(
            src_ref=y_b.at[b, pl.ds(i * CAP, CAP)],
            dst_ref=ret.at[pl.ds(pl.multiple_of(ep * CAP, CAP), CAP)],
            send_sem=ret_s.at[b, i],
            recv_sem=ret_r.at[b, i],
            device_id=(target, tp),
            device_id_type=MESH,
        )

    def expert_result(b):
        out_t = nn(down_t[...], hs[b]).astype(BF16)
        identity = jnp.where(eye(256), 1.0, 0.0).astype(BF16)
        y_b[b] = nt(identity, out_t).astype(BF16)
        for i, o in enumerate(GROUPS[b]):
            if o != (0, 0):
                give_back(b, i).start()
            else:
                ret[pl.ds(pl.multiple_of(ep * CAP, CAP), CAP), :] = y_b[b, i * CAP : (i + 1) * CAP, :]

    def mixed_result():
        mixed_t = nn(mout_t[...], grouped[...]).astype(BF16)
        identity = jnp.where(eye(128), 1.0, 0.0).astype(BF16)
        mixed_o[...] = nt(identity, mixed_t).astype(BF16)

    def wait_weights():
        loads["gate"].wait()
        loads["up"].wait()

    tasks = []

    def at(slot_time, *calls):
        tasks.append((slot_time, len(tasks), calls))

    def gather_at(start, spacing, gather, before_calls, after_calls, gap):
        at(start, *before_calls, gather.first)
        for k in range(1, 5):
            at(start + spacing * k, functools.partial(gather.step, k))
        at(start + spacing * 4 + gap, gather.finish, *after_calls)

    at(0.1, wait_weights)
    at(0.2, prepare_combine)
    at(1.1, prepare_down)
    for b in range(BATCHES):
        way = 1 if b % 2 == 0 else -1
        gather_at(
            4 * b, 3, Gather(b, "x", b, way),
            [functools.partial(wait_dispatched, b)], [functools.partial(hidden, b)], 1.5,
        )
        gather_at(
            4 * (BATCHES + b), 3, Gather(BATCHES + b, "h", b, way),
            [], [functools.partial(expert_result, b)], 1.5,
        )
    gather_at(5.2, 3, Gather(2 * BATCHES, "m", 0, 1), [mixer_group], [mixed_result], 1.5)
    for _, _, calls in sorted(tasks, key=lambda task: task[:2]):
        for call in calls:
            call()

    for b in range(BATCHES):
        for i, o in enumerate(GROUPS[b]):
            if o != (0, 0):
                dz, dx = o
                source = ep_at(-dz, -dx)
                pltpu.make_async_remote_copy(
                    src_ref=y_b.at[b, pl.ds(i * CAP, CAP)],
                    dst_ref=ret.at[pl.ds(pl.multiple_of(source * CAP, CAP), CAP)],
                    send_sem=ret_s.at[b, i],
                    recv_sem=ret_r.at[b, i],
                    device_id=(source, tp),
                    device_id_type=MESH,
                ).wait_recv()
    results = ret[...]
    tokens_o[...] = (nn(combine[0], results) + nn(combine[1], results)).astype(BF16)

    for copy in started:
        copy.wait_send()
    for b in range(BATCHES):
        for i, o in enumerate(GROUPS[b]):
            if o != (0, 0):
                dispatch(b, i).wait_send()
                give_back(b, i).wait_send()


def per_device(
    mixer_input, mixer_gain, outer_weight, inner_weight, value_weight, conv_kernel, group_gain,
    mixer_out_weight, expert_input, expert_gain, routes, route_weight, expert_gate, expert_up,
    expert_down,
):
    phases = 2 * BATCHES + 1
    vmem = pltpu.VMEM
    dma = pltpu.SemaphoreType.DMA
    return pl.pallas_call(
        kernel,
        name="mixer_and_experts",
        out_shape=(
            jax.ShapeDtypeStruct((128, 128), BF16),
            jax.ShapeDtypeStruct((256, 128), BF16),
        ),
        in_specs=[pl.BlockSpec(memory_space=pl.ANY)] * 15,
        out_specs=(pl.BlockSpec(memory_space=vmem), pl.BlockSpec(memory_space=vmem)),
        scratch_shapes=[
            vmem((128, 2048), BF16),
            vmem((1, 2048), F32),
            vmem((192, 2048), BF16),
            vmem((3, 64), BF16),
            vmem((1, 64), F32),
            vmem((1024, 128), BF16),
            vmem((256, 2048), BF16),
            vmem((1, 2048), F32),
            vmem((2, 256), jnp.int32),
            vmem((2, 256), F32),
            vmem((448, 2048), BF16),
            vmem((3584, 128), BF16),
            vmem((1024, 256), BF16),
            vmem((N_EP, 256), F32),
            vmem((N_EP, 256), F32),
            vmem((2, 256, 1024), BF16),
            vmem((1024, 256), BF16),
            vmem((1024, 128), BF16),
            vmem((BATCHES, 256, 2048), BF16),
            vmem((BATCHES, 3584, 256), BF16),
            vmem((BATCHES, 256, 128), BF16),
            vmem((1024, 128), BF16),
            vmem((128, 3584), BF16),
            vmem((128, 1024), BF16),
            vmem((1024, 128), BF16),
            vmem((64, 128), F32),
            vmem((64, 128), F32),
            vmem((64, 128), F32),
            dma((15,)),
            dma((BATCHES, PER)),
            dma((BATCHES, PER)),
            dma((BATCHES, PER)),
            dma((BATCHES, PER)),
            dma((phases, 7)),
            dma((phases, 7)),
            dma((phases, 8)),
            dma((phases, 8)),
            dma((2,)),
        ],
        compiler_params=pltpu.CompilerParams(
            collective_id=0, has_side_effects=True, vmem_limit_bytes=56 * 1024 * 1024
        ),
    )(
        mixer_input, mixer_gain.reshape(1, -1), outer_weight.T, inner_weight.T, value_weight.T,
        conv_kernel, group_gain.reshape(1, -1), mixer_out_weight, expert_input,
        expert_gain.reshape(1, -1), routes.T, route_weight.T, expert_gate[0].T, expert_up[0].T,
        expert_down[0],
    )


def solution(mesh):
    placed = (
        P("ep", None), P(), P(None, "tp"), P(None, "tp"), P(None, "tp"), P(None, "tp"), P("tp"),
        P(None, "tp"), P("ep", None), P(), P("ep", None), P("ep", None), P("ep", None, "tp"),
        P("ep", None, "tp"), P("ep", None, "tp"),
    )
    return jax.shard_map(
        per_device,
        mesh=mesh,
        in_specs=placed,
        out_specs=(P("ep", "tp"), P("ep", "tp")),
        check_vma=False,
    )
```

time: 201 us -> 101 us (0.50)
  waiting for transfers between devices: 107 us -> 0 us
  Pallas kernels: 0 us -> 97.9 us
  blocking collectives: 24.9 us -> 0 us
  starting transfers between devices: 17.8 us -> 0 us
  matrix products: 13.9 us -> 0 us
  between operations: 14.4 us -> 0.65 us
  local copies, waits for them, and re-layouts: 13 us -> 2.04 us
  other arithmetic: 8.83 us -> 0 us
    pallas_call x0 -> x1, Pallas kernels: none -> 97.9 us  [per_device(): pl.pallas_call(kernel, name='mixer_and_experts', out_shape=(jax.ShapeDtyp...]
    all_gather x2 -> x0, waiting for transfers between devices: 96.1 us -> none  [the longest x1 50.3 us: per_device(): piece = lax.all_gather(received, 'tp', axis=2, tiled=True)]
    all_to_all x1 -> x0, blocking collectives: 24.9 us -> none  [per_device(): lax.all_to_all(outgoing, 'ep', split_axis=0, concat_axis=0, tiled=True)]
    all_to_all x2 -> x0, starting transfers between devices: 15.5 us -> none  [the longest x1 10.1 us: per_device(): lax.all_to_all(results.reshape(sources, count, out_cols), 'ep', split_axi...]
    dot_general x7 -> x0, matrix products: 13.9 us -> none  [the longest x1 5.91 us: per_device(): jnp.dot(lax.all_gather(hidden, 'tp', axis=1, tiled=True), weight_rows, pr...]
    all_to_all x2 -> x0, waiting for transfers between devices: 10.4 us -> none  [the longest x1 10.4 us: per_device(): lax.all_to_all(results.reshape(sources, count, out_cols), 'ep', split_axi...]
    gather x2 -> x0, local copies, waits for them, and re-layouts: 7.31 us -> none  [the longest x1 5.98 us: per_device(): gathered_rows = jnp.take(normed_b, jnp.maximum(table - 1, 0), axis=0)]
    reduce_sum x4 -> x0, other arithmetic: 3.88 us -> none  [the longest x1 2.08 us: per_device(): weighted = jnp.sum(chosen * route_weight[..., None], axis=1)]
  transfers between devices with their start and end apart: 5 -> 0, of which waited for: 4 -> 0; matrix products, arithmetic and copies ran while one was open for 5% -> 0% of each run, Pallas kernels for 0% -> 0%
where the time goes in v1:
time: 101 us
  Pallas kernels  97.9 us (97%)
  local copies, waits for them, and re-layouts  2.04 us (2%)
    pallas_call x1, Pallas kernels, per_device(): pl.pallas_call(kernel, name='mixer_and_experts', out_shape=(jax.ShapeDtyp...  97.9 us
    unnamed x4, local copies, waits for them, and re-layouts  2.04 us

profile of v1, /device:TPU:1, one launch (start us, length us, event | category | flops | bytes accessed | tf_op | source)
XLA Modules:
  0.0 100.6 jit_solution(16727215996481796505)
XLA Ops:
  0.6 97.9 %mixer_and_experts.1 = (bf16[128,128]{1,0:T(8,128)(2,1)}, bf16[256,128]{1,0:T(8,128)(2,1)}) custom-call(bf16[128,2048]{1,0:T(8,128)(2,1)} %mixin_h.1, f32[1,2048]{1,0:T(1,128)} %bitcast.21, bf16[64,2048]{1,0:T(8,128)(2,1)} %bitcast.18, bf16[64,2048]{1,0:T(8,128)(2,1)} %bitcast.19, bf16[64,2048]{1,0:T(8,128)(2,1)} %bitcast.20, bf16[3,64]{1,0:T(4,128)(2,1)} %conv_h.1, ...), custom_call_target="tpu_custom_call" | custom-call | tf_op jit(solution)/shard_map/mixer_and_experts/pallas_call | solution.py:375
  98.5 0.0 copy-start
  98.5 1.4 %copy.19 = bf16[128,128]{1,0:T(8,128)(2,1)} copy(bf16[128,128]{1,0:T(8,128)(2,1)} %get-tuple-element.4) | data formatting | bytes 65536
  99.9 0.0 copy-done
  99.9 0.6 copy.20
Async XLA Ops:
  98.5 1.4 %copy-start = (bf16[256,128]{1,0:T(8,128)(2,1)S(1)}, bf16[256,128]{1,0:T(8,128)(2,1)}, u32[]{:S(2)}) copy-start(bf16[256,128]{1,0:T(8,128)(2,1)} %get-tuple-element.5) | copy-start | bytes 196612

commit v2 on v1

--- a/solution.py
+++ b/solution.py
@@ -16,21 +16,31 @@
 N_Y = 8
 N_TP = 2 * N_Y
 BATCHES = 4
+EARLY = 2
+ROWS, HIDDEN, MIXER = "x", "h", "m"
+END = 9
+ORDER = (
+    (ROWS, 0, 0), (ROWS, 1, 0), (ROWS, 0, 1), (ROWS, 0, 2), (ROWS, 1, 1), (ROWS, 2, 0),
+    (ROWS, 1, 2), (ROWS, 0, 3), (ROWS, 0, END), (ROWS, 1, 3), (MIXER, 0, 0), (ROWS, 2, 1),
+    (ROWS, 1, END), (ROWS, 2, 2), (HIDDEN, 1, 0), (ROWS, 2, 3), (ROWS, 3, 0), (ROWS, 2, END),
+    (MIXER, 0, 1), (HIDDEN, 1, 1), (ROWS, 3, 1), (ROWS, 3, 2), (HIDDEN, 1, 2), (MIXER, 0, 2),
+    (ROWS, 3, 3), (ROWS, 3, END), (HIDDEN, 3, 0), (HIDDEN, 2, 0), (HIDDEN, 1, 3), (MIXER, 0, 3),
+    (HIDDEN, 3, 1), (HIDDEN, 0, 0), (HIDDEN, 2, 1), (HIDDEN, 1, 4), (HIDDEN, 1, END), (HIDDEN, 3, 2),
+    (MIXER, 0, 4), (HIDDEN, 0, 1), (MIXER, 0, END), (HIDDEN, 2, 2), (HIDDEN, 3, 3), (HIDDEN, 0, 2),
+    (HIDDEN, 2, 3), (HIDDEN, 3, 4), (HIDDEN, 3, END), (HIDDEN, 0, 3), (HIDDEN, 2, 4), (HIDDEN, 2, END),
+    (HIDDEN, 0, 4), (HIDDEN, 0, END),
+)
 CAP = 32
 PER = N_EP // BATCHES
 
 
-def hops(n, d):
-    return min(d, n - d)
-
-
-def offset_order():
-    pairs = [(dz, dx) for dz in range(NZ) for dx in range(NX)]
-    return sorted(pairs, key=lambda o: (hops(NZ, o[0]) + hops(NX, o[1]), hops(NZ, o[0]), o))
-
-
-OFFSETS = offset_order()
-GROUPS = [OFFSETS[8:16], OFFSETS[16:24], OFFSETS[24:32], OFFSETS[0:8]]
+GROUPS = (
+    ((0, 0), (0, 1), (0, 2), (0, 3), (1, 0), (1, 1), (7, 0), (7, 3)),
+    ((1, 2), (1, 3), (7, 1), (7, 2), (2, 0), (2, 1), (6, 0), (6, 3)),
+    ((2, 2), (2, 3), (6, 1), (6, 2), (3, 0), (3, 1), (5, 0), (5, 3)),
+    ((3, 2), (3, 3), (5, 1), (5, 2), (4, 0), (4, 1), (4, 2), (4, 3)),
+)
+COPIES = (2, 2, 2, 2)
 
 
 def nt(a, b):
@@ -59,7 +69,7 @@
     expin, egain, routes, rweight, gateup, down,
     onehot, pos32, wsel32, combine, wide_t, send_b, xs, hs, y_b, ret,
     down_t, mout_t, grouped, prod_s, halo, outer_s,
-    load_sem, disp_s, disp_r, ret_s, ret_r, ring_s, ring_r, part_s, part_r, halo_sem,
+    load_sem, disp_s, disp_r, ret_s, ret_r, sent, ring_r, part_r, halo_sem,
 ):
     ep = lax.axis_index("ep")
     tp = lax.axis_index("tp")
@@ -74,31 +84,38 @@
     def ring_tp(d):
         return lax.rem(tp + 2 * d + N_TP, N_TP)
 
-    loads = {}
-    for i, (name, src, dst) in enumerate(
-        [
-            ("routes", routes_h, routes),
-            ("expin", expin_h, expin),
-            ("egain", egain_h, egain),
-            ("mixin", mixin_h, mixin),
-            ("mgain", mgain_h, mgain),
-            ("outer", outer_h, mproj.at[pl.ds(0, 64)]),
-            ("inner", inner_h, mproj.at[pl.ds(64, 64)]),
-            ("value", value_h, mproj.at[pl.ds(128, 64)]),
-            ("conv", conv_h, conv),
-            ("ggain", ggain_h, ggain),
-            ("rweight", rweight_h, rweight),
-            ("gate", gate_h, gateup.at[pl.ds(0, 224)]),
-            ("up", up_h, gateup.at[pl.ds(224, 224)]),
-            ("down", down_h, down),
-            ("mout", mout_h, mout),
-        ]
-    ):
-        loads[name] = pltpu.make_async_copy(src, dst, load_sem.at[i])
+    across = ring_tp(N_Y // 2)
+
+    def features(j):
+        return pl.ds(pl.multiple_of(j * 128, 128), 128)
+
+    sources = dict(
+        routes=(routes_h, routes),
+        expin=(expin_h, expin),
+        egain=(egain_h, egain),
+        mixin=(mixin_h, mixin),
+        mgain=(mgain_h, mgain),
+        outer=(outer_h, mproj.at[pl.ds(0, 64)]),
+        inner=(inner_h, mproj.at[pl.ds(64, 64)]),
+        value=(value_h, mproj.at[pl.ds(128, 64)]),
+        conv=(conv_h, conv),
+        ggain=(ggain_h, ggain),
+        rweight=(rweight_h, rweight),
+        gate=(gate_h, gateup.at[pl.ds(0, 224)]),
+        up=(up_h, gateup.at[pl.ds(224, 224)]),
+        down=(down_h, down),
+        mout=(mout_h, mout),
+    )
+    loads = {
+        name: pltpu.make_async_copy(src, dst, load_sem.at[i])
+        for i, (name, (src, dst)) in enumerate(sources.items())
+    }
+    urgent = ("routes", "expin", "egain")
+    for name in urgent:
         loads[name].start()
 
     barrier = pltpu.get_barrier_semaphore()
-    for dz, dx in OFFSETS[1:]:
+    for dz, dx in (o for group in GROUPS for o in group if o != (0, 0)):
         pl.semaphore_signal(barrier, inc=1, device_id=(ep_at(dz, dx), tp), device_id_type=MESH)
     for other in (ring_tp(1), ring_tp(-1), mate):
         pl.semaphore_signal(barrier, inc=1, device_id=(ep, other), device_id_type=MESH)
@@ -121,34 +138,47 @@
 
     loads["expin"].wait()
     loads["egain"].wait()
-    own_features = pl.ds(pl.multiple_of(tp * 128, 128), 128)
+    for name in loads:
+        if name not in urgent:
+            loads[name].start()
     rows = expin[...].astype(F32)
     scale = lax.rsqrt(jnp.mean(rows * rows, axis=-1, keepdims=True) + EPS)
-    normed_b = (expin[:, own_features].astype(F32) * scale * egain[:, own_features]).astype(BF16)
-    send_b[...] = nn(onehot[...], normed_b).astype(BF16)
+    normed_b = jnp.concatenate(
+        [
+            (expin[:, part].astype(F32) * scale * egain[:, part]).astype(BF16)
+            for part in (features(tp), features(across))
+        ],
+        axis=1,
+    )
+    both_parts = nn(onehot[...], normed_b).astype(BF16)
+    send_b[0], send_b[1] = both_parts[:, :128], both_parts[:, 128:]
 
     pl.semaphore_wait(barrier, N_EP - 1 + 3)
 
-    def dispatch(b, i):
+    def dispatch(b, i, part):
         dz, dx = GROUPS[b][i]
         target = ep_at(-dz, -dx)
         return pltpu.make_async_remote_copy(
-            src_ref=send_b.at[pl.ds(pl.multiple_of(target * CAP, CAP), CAP)],
-            dst_ref=xs.at[b, pl.ds(i * CAP, CAP), own_features],
-            send_sem=disp_s.at[b, i],
-            recv_sem=disp_r.at[b, i],
+            src_ref=send_b.at[part, pl.ds(pl.multiple_of(target * CAP, CAP), CAP)],
+            dst_ref=xs.at[b, pl.ds(i * CAP, CAP), features((tp, across)[part])],
+            send_sem=disp_s.at[0],
+            recv_sem=disp_r.at[b],
             device_id=(target, tp),
             device_id_type=MESH,
         )
 
-    for b in range(BATCHES):
+    def dispatch_batch(b):
         for i, o in enumerate(GROUPS[b]):
-            if o != (0, 0):
-                dispatch(b, i).start()
-            else:
-                xs[b, i * CAP : (i + 1) * CAP, own_features] = send_b[
-                    pl.ds(pl.multiple_of(ep * CAP, CAP), CAP), :
-                ]
+            for part, chunk in enumerate((tp, across)[: COPIES[b]]):
+                if o != (0, 0):
+                    dispatch(b, i, part).start()
+                else:
+                    xs[b, i * CAP : (i + 1) * CAP, features(chunk)] = send_b[
+                        part, pl.ds(pl.multiple_of(ep * CAP, CAP), CAP), :
+                    ]
+
+    for b in range(EARLY):
+        dispatch_batch(b)
 
     for name in ("mixin", "mgain", "outer", "inner", "value"):
         loads[name].wait()
@@ -168,6 +198,8 @@
         device_id_type=MESH,
     )
     halo_copy.start()
+    for b in range(EARLY, BATCHES):
+        dispatch_batch(b)
 
     def mixer_group():
         halo_copy.wait()
@@ -207,13 +239,33 @@
         mout_t[...] = nt(identity, mout[...]).astype(BF16)
 
     def piece_of(kind, b):
-        if kind == "x":
-            return lambda j: xs.at[b, :, pl.ds(pl.multiple_of(j * 128, 128), 128)]
-        if kind == "h":
-            return lambda j: hs.at[b, pl.ds(pl.multiple_of(j * 224, 224), 224)]
-        return lambda j: grouped.at[pl.ds(pl.multiple_of(j * 64, 64), 64)]
-
-    started = []
+        if kind == ROWS:
+            return lambda j, h=0, n=1: xs.at[b, pl.ds(h * 128, 256 // n), features(j)]
+        if kind == HIDDEN:
+            return lambda j, h=0, n=1: hs.at[b, pl.ds(pl.multiple_of(j * 224 + h * 112, 16), 224 // n)]
+        return lambda j, h=0, n=1: grouped.at[pl.ds(pl.multiple_of(j * 64 + h * 32, 32), 64 // n)]
+
+    def part_of(kind, b):
+        if kind == ROWS:
+            return lambda n: xs.at[b, :, pl.ds(0, n * 128)]
+        if kind == HIDDEN:
+            return lambda n: hs.at[b, pl.ds(0, n * 224)]
+        return lambda n: grouped.at[pl.ds(0, n * 64)]
+
+    def arrived(ref, sem):
+        pltpu.make_async_remote_copy(
+            src_ref=ref, dst_ref=ref, send_sem=disp_s.at[0], recv_sem=sem,
+            device_id=(ep, mate), device_id_type=MESH,
+        ).wait_recv()
+
+    def left(ref, sem):
+        pltpu.make_async_remote_copy(
+            src_ref=ref, dst_ref=ref, send_sem=sem, recv_sem=disp_r.at[0],
+            device_id=(ep, mate), device_id_type=MESH,
+        ).wait_send()
+
+    def remote_rows(b):
+        return CAP * sum(o != (0, 0) for o in GROUPS[b])
 
     def send(src, dst, send_sem, recv_sem, to):
         copy = pltpu.make_async_remote_copy(
@@ -221,57 +273,62 @@
             device_id=(ep, to), device_id_type=MESH,
         )
         copy.start()
-        started.append(copy)
 
     class Gather:
-        def __init__(self, number, kind, b, far):
-            self.n, self.piece = number, piece_of(kind, b)
-            self.reach = {1: 4 if far > 0 else 3, -1: 4 if far < 0 else 3}
-
-        def index(self, way, k):
-            return k - 1 if way == 1 else self.reach[1] + k - 1
+        def __init__(self, number, kind, b):
+            self.n, self.piece, self.part = number, piece_of(kind, b), part_of(kind, b)
+
+        def received(self, way, k):
+            return ring_r.at[self.n, (k if way == 1 else 4 + k) - 1]
 
         def on_ring(self, ref, way, k):
-            i = self.index(way, k)
-            send(ref, ref, ring_s.at[self.n, i], ring_r.at[self.n, i], ring_tp(way))
-
-        def to_mate(self, ref, i):
-            send(ref, ref, part_s.at[self.n, i], part_r.at[self.n, i], mate)
-
-        def wait(self, ref, sem):
-            pltpu.make_async_remote_copy(
-                src_ref=ref, dst_ref=ref, send_sem=part_s.at[self.n, 0], recv_sem=sem,
-                device_id=(ep, mate), device_id_type=MESH,
-            ).wait_recv()
+            send(ref, ref, sent.at[self.n], self.received(way, k), ring_tp(way))
+
+        def to_mate(self, ref):
+            send(ref, ref, sent.at[self.n], part_r.at[self.n], mate)
 
         def first(self):
             ref = self.piece(tp)
             self.on_ring(ref, 1, 1)
             self.on_ring(ref, -1, 1)
-            self.to_mate(ref, 7)
+            self.to_mate(ref)
+
+        def step(self, k):
+            for way, h in ((1, 0), (-1, 1)):
+                j = ring_tp(-way * k)
+                ref = self.piece(j) if k < 4 else self.piece(j, h, 2)
+                arrived(ref, self.received(way, k))
+                if k < 4:
+                    self.on_ring(ref if k < 3 else self.piece(j, h, 2), way, k + 1)
+                self.to_mate(ref)
+
+        def finish(self):
+            arrived(self.part(N_Y), part_r.at[self.n])
+
+        def all_sent(self):
+            left(self.part(N_TP - 1), sent.at[self.n])
+
+    class PairGather(Gather):
+        def first(self):
+            for k, j in enumerate((tp, across)):
+                ref = self.piece(j)
+                self.on_ring(ref, 1, 1 + k)
+                self.on_ring(ref, -1, 1 + k)
+                self.to_mate(ref)
 
         def step(self, k):
             for way in (1, -1):
-                if k > self.reach[way]:
-                    continue
-                ref = self.piece(ring_tp(-way * k))
-                i = self.index(way, k)
-                self.wait(ref, ring_r.at[self.n, i])
-                if k < self.reach[way]:
-                    self.on_ring(ref, way, k + 1)
-                self.to_mate(ref, i)
-
-        def finish(self):
-            self.wait(self.piece(mate), part_r.at[self.n, 7])
-            for way in (1, -1):
-                for k in range(1, self.reach[way] + 1):
-                    j = lax.rem(mate - 2 * way * k + N_TP, N_TP)
-                    self.wait(self.piece(j), part_r.at[self.n, self.index(way, k)])
+                ref = self.piece(ring_tp((-way, 3 * way, -2 * way)[k - 1]))
+                arrived(ref, self.received(way, k))
+                if k == 1:
+                    self.on_ring(ref, way, 3)
+                self.to_mate(ref)
+
+        def all_sent(self):
+            left(self.part(N_TP - 2), sent.at[self.n])
 
     def wait_dispatched(b):
-        for i, o in enumerate(GROUPS[b]):
-            if o != (0, 0):
-                dispatch(b, i).wait_recv()
+        arrived(xs.at[b, pl.ds(0, remote_rows(b)), pl.ds(0, 128 * COPIES[b])], disp_r.at[b])
 
     def hidden(b):
         both = nt(gateup[...], xs[b])
@@ -285,8 +342,8 @@
         return pltpu.make_async_remote_copy(
             src_ref=y_b.at[b, pl.ds(i * CAP, CAP)],
             dst_ref=ret.at[pl.ds(pl.multiple_of(ep * CAP, CAP), CAP)],
-            send_sem=ret_s.at[b, i],
-            recv_sem=ret_r.at[b, i],
+            send_sem=ret_s.at[0],
+            recv_sem=ret_r.at[0],
             device_id=(target, tp),
             device_id_type=MESH,
         )
@@ -310,58 +367,46 @@
         loads["gate"].wait()
         loads["up"].wait()
 
-    tasks = []
-
-    def at(slot_time, *calls):
-        tasks.append((slot_time, len(tasks), calls))
-
-    def gather_at(start, spacing, gather, before_calls, after_calls, gap):
-        at(start, *before_calls, gather.first)
-        for k in range(1, 5):
-            at(start + spacing * k, functools.partial(gather.step, k))
-        at(start + spacing * 4 + gap, gather.finish, *after_calls)
-
-    at(0.1, wait_weights)
-    at(0.2, prepare_combine)
-    at(1.1, prepare_down)
+    gathers = {(MIXER, 0): Gather(2 * BATCHES, MIXER, 0)}
     for b in range(BATCHES):
-        way = 1 if b % 2 == 0 else -1
-        gather_at(
-            4 * b, 3, Gather(b, "x", b, way),
-            [functools.partial(wait_dispatched, b)], [functools.partial(hidden, b)], 1.5,
-        )
-        gather_at(
-            4 * (BATCHES + b), 3, Gather(BATCHES + b, "h", b, way),
-            [], [functools.partial(expert_result, b)], 1.5,
-        )
-    gather_at(5.2, 3, Gather(2 * BATCHES, "m", 0, 1), [mixer_group], [mixed_result], 1.5)
-    for _, _, calls in sorted(tasks, key=lambda task: task[:2]):
-        for call in calls:
-            call()
-
-    for b in range(BATCHES):
-        for i, o in enumerate(GROUPS[b]):
-            if o != (0, 0):
-                dz, dx = o
-                source = ep_at(-dz, -dx)
-                pltpu.make_async_remote_copy(
-                    src_ref=y_b.at[b, pl.ds(i * CAP, CAP)],
-                    dst_ref=ret.at[pl.ds(pl.multiple_of(source * CAP, CAP), CAP)],
-                    send_sem=ret_s.at[b, i],
-                    recv_sem=ret_r.at[b, i],
-                    device_id=(source, tp),
-                    device_id_type=MESH,
-                ).wait_recv()
+        gathers[ROWS, b] = (PairGather if COPIES[b] == 2 else Gather)(b, ROWS, b)
+        gathers[HIDDEN, b] = Gather(BATCHES + b, HIDDEN, b)
+
+    for kind, b, step in ORDER:
+        gather = gathers[kind, b]
+        if step == 0:
+            if kind == ROWS:
+                wait_dispatched(b)
+            elif kind == MIXER:
+                mixer_group()
+            gather.first()
+            if kind == ROWS and b == 0:
+                wait_weights()
+                prepare_combine()
+            elif kind == ROWS and b == 1:
+                prepare_down()
+        elif step < END:
+            gather.step(step)
+        else:
+            gather.finish()
+            if kind == ROWS:
+                hidden(b)
+            elif kind == HIDDEN:
+                expert_result(b)
+            else:
+                mixed_result()
+
+    others = (N_EP - 1) * CAP
+    arrived(ret.at[pl.ds(0, others)], ret_r.at[0])
     results = ret[...]
     tokens_o[...] = (nn(combine[0], results) + nn(combine[1], results)).astype(BF16)
 
-    for copy in started:
-        copy.wait_send()
+    for gather in gathers.values():
+        gather.all_sent()
     for b in range(BATCHES):
-        for i, o in enumerate(GROUPS[b]):
-            if o != (0, 0):
-                dispatch(b, i).wait_send()
-                give_back(b, i).wait_send()
+        for _ in range(COPIES[b]):
+            left(send_b.at[0, pl.ds(0, remote_rows(b))], disp_s.at[0])
+    left(ret.at[pl.ds(0, others)], ret_s.at[0])
 
 
 def per_device(
@@ -399,7 +444,7 @@
             vmem((N_EP, 256), F32),
             vmem((2, 256, 1024), BF16),
             vmem((1024, 256), BF16),
-            vmem((1024, 128), BF16),
+            vmem((2, 1024, 128), BF16),
             vmem((BATCHES, 256, 2048), BF16),
             vmem((BATCHES, 3584, 256), BF16),
             vmem((BATCHES, 256, 128), BF16),
@@ -411,14 +456,13 @@
             vmem((64, 128), F32),
             vmem((64, 128), F32),
             dma((15,)),
-            dma((BATCHES, PER)),
-            dma((BATCHES, PER)),
-            dma((BATCHES, PER)),
-            dma((BATCHES, PER)),
-            dma((phases, 7)),
-            dma((phases, 7)),
+            dma((1,)),
+            dma((BATCHES,)),
+            dma((1,)),
+            dma((1,)),
+            dma((phases,)),
             dma((phases, 8)),
-            dma((phases, 8)),
+            dma((phases,)),
             dma((2,)),
         ],
         compiler_params=pltpu.CompilerParams(

time: 101 us -> 91 us (0.901)
  Pallas kernels: 97.9 us -> 88.2 us
    pallas_call x1, Pallas kernels: 97.9 us -> 88.2 us  [per_device(): pl.pallas_call(kernel, name='mixer_and_experts', out_shape=(jax.ShapeDtyp...]
where the time goes in v2:
time: 91 us; the launch traced here: 90.8 us
  Pallas kernels  88.2 us (97%)
  local copies, waits for them, and re-layouts  2.04 us (2%)
    pallas_call x1, Pallas kernels, per_device(): pl.pallas_call(kernel, name='mixer_and_experts', out_shape=(jax.ShapeDtyp...  88.2 us
    unnamed x4, local copies, waits for them, and re-layouts  2.04 us

profile of v2, /device:TPU:1, one launch (start us, length us, event | category | flops | bytes accessed | tf_op | source)
XLA Modules:
  0.0 90.8 jit_solution(15008379267444401927)
XLA Ops:
  0.6 88.2 %mixer_and_experts.1 = (bf16[128,128]{1,0:T(8,128)(2,1)}, bf16[256,128]{1,0:T(8,128)(2,1)}) custom-call(bf16[128,2048]{1,0:T(8,128)(2,1)} %mixin_h.1, f32[1,2048]{1,0:T(1,128)} %bitcast.21, bf16[64,2048]{1,0:T(8,128)(2,1)} %bitcast.18, bf16[64,2048]{1,0:T(8,128)(2,1)} %bitcast.19, bf16[64,2048]{1,0:T(8,128)(2,1)} %bitcast.20, bf16[3,64]{1,0:T(4,128)(2,1)} %conv_h.1, ...), custom_call_target="tpu_custom_call" | custom-call | tf_op jit(solution)/shard_map/mixer_and_experts/pallas_call | solution.py:420
  88.8 0.0 copy-start
  88.8 1.4 %copy.19 = bf16[128,128]{1,0:T(8,128)(2,1)} copy(bf16[128,128]{1,0:T(8,128)(2,1)} %get-tuple-element.4) | data formatting | bytes 65536
  90.2 0.0 copy-done
  90.2 0.6 copy.20
Async XLA Ops:
  88.8 1.4 %copy-start = (bf16[256,128]{1,0:T(8,128)(2,1)S(1)}, bf16[256,128]{1,0:T(8,128)(2,1)}, u32[]{:S(2)}) copy-start(bf16[256,128]{1,0:T(8,128)(2,1)} %get-tuple-element.5) | copy-start | bytes 196612

commit v3 on v2

--- a/solution.py
+++ b/solution.py
@@ -20,25 +20,25 @@
 ROWS, HIDDEN, MIXER = "x", "h", "m"
 END = 9
 ORDER = (
-    (ROWS, 0, 0), (ROWS, 1, 0), (ROWS, 0, 1), (ROWS, 0, 2), (ROWS, 1, 1), (ROWS, 2, 0),
-    (ROWS, 1, 2), (ROWS, 0, 3), (ROWS, 0, END), (ROWS, 1, 3), (MIXER, 0, 0), (ROWS, 2, 1),
-    (ROWS, 1, END), (ROWS, 2, 2), (HIDDEN, 1, 0), (ROWS, 2, 3), (ROWS, 3, 0), (ROWS, 2, END),
-    (MIXER, 0, 1), (HIDDEN, 1, 1), (ROWS, 3, 1), (ROWS, 3, 2), (HIDDEN, 1, 2), (MIXER, 0, 2),
-    (ROWS, 3, 3), (ROWS, 3, END), (HIDDEN, 3, 0), (HIDDEN, 2, 0), (HIDDEN, 1, 3), (MIXER, 0, 3),
-    (HIDDEN, 3, 1), (HIDDEN, 0, 0), (HIDDEN, 2, 1), (HIDDEN, 1, 4), (HIDDEN, 1, END), (HIDDEN, 3, 2),
-    (MIXER, 0, 4), (HIDDEN, 0, 1), (MIXER, 0, END), (HIDDEN, 2, 2), (HIDDEN, 3, 3), (HIDDEN, 0, 2),
-    (HIDDEN, 2, 3), (HIDDEN, 3, 4), (HIDDEN, 3, END), (HIDDEN, 0, 3), (HIDDEN, 2, 4), (HIDDEN, 2, END),
-    (HIDDEN, 0, 4), (HIDDEN, 0, END),
+    (ROWS, 0, 0), (ROWS, 1, 0), (ROWS, 0, 1), (ROWS, 1, 1), (ROWS, 0, 2), (ROWS, 2, 0),
+    (ROWS, 1, 2), (ROWS, 3, 0), (ROWS, 1, 3), (ROWS, 2, 1), (ROWS, 1, END), (ROWS, 0, 3),
+    (ROWS, 3, 1), (ROWS, 2, 2), (HIDDEN, 1, 0), (ROWS, 0, END), (HIDDEN, 0, 0), (ROWS, 3, 2),
+    (ROWS, 2, 3), (ROWS, 2, END), (ROWS, 3, 3), (HIDDEN, 2, 0), (ROWS, 3, END), (HIDDEN, 3, 0),
+    (HIDDEN, 1, 1), (HIDDEN, 2, 1), (HIDDEN, 3, 1), (MIXER, 0, 0), (HIDDEN, 1, 2), (HIDDEN, 3, 2),
+    (HIDDEN, 0, 1), (HIDDEN, 2, 2), (HIDDEN, 3, 3), (HIDDEN, 0, 2), (MIXER, 0, 1), (HIDDEN, 2, 3),
+    (HIDDEN, 1, 3), (HIDDEN, 3, 4), (HIDDEN, 0, 3), (HIDDEN, 3, END), (HIDDEN, 2, 4), (MIXER, 0, 2),
+    (HIDDEN, 1, 4), (HIDDEN, 2, END), (HIDDEN, 0, 4), (HIDDEN, 1, END), (MIXER, 0, 3), (HIDDEN, 0, END),
+    (MIXER, 0, 4), (MIXER, 0, END),
 )
 CAP = 32
 PER = N_EP // BATCHES
 
 
 GROUPS = (
-    ((0, 0), (0, 1), (0, 2), (0, 3), (1, 0), (1, 1), (7, 0), (7, 3)),
-    ((1, 2), (1, 3), (7, 1), (7, 2), (2, 0), (2, 1), (6, 0), (6, 3)),
-    ((2, 2), (2, 3), (6, 1), (6, 2), (3, 0), (3, 1), (5, 0), (5, 3)),
-    ((3, 2), (3, 3), (5, 1), (5, 2), (4, 0), (4, 1), (4, 2), (4, 3)),
+    ((1, 0), (7, 0), (0, 1), (0, 3), (1, 1), (7, 3), (0, 2), (0, 0)),
+    ((2, 0), (6, 0), (1, 3), (7, 1), (2, 1), (6, 3), (1, 2), (7, 2)),
+    ((2, 2), (6, 2), (3, 0), (5, 0), (2, 3), (6, 1), (3, 1), (5, 3)),
+    ((4, 0), (5, 1), (3, 3), (4, 1), (5, 2), (3, 2), (4, 3), (4, 2)),
 )
 COPIES = (2, 2, 2, 2)
 
@@ -85,9 +85,13 @@
         return lax.rem(tp + 2 * d + N_TP, N_TP)
 
     across = ring_tp(N_Y // 2)
+    low = lax.rem(tp, N_Y)
 
     def features(j):
         return pl.ds(pl.multiple_of(j * 128, 128), 128)
+
+    def place(j):
+        return features(2 * lax.rem(j, N_Y) + j // N_Y)
 
     sources = dict(
         routes=(routes_h, routes),
@@ -101,8 +105,6 @@
         conv=(conv_h, conv),
         ggain=(ggain_h, ggain),
         rweight=(rweight_h, rweight),
-        gate=(gate_h, gateup.at[pl.ds(0, 224)]),
-        up=(up_h, gateup.at[pl.ds(224, 224)]),
         down=(down_h, down),
         mout=(mout_h, mout),
     )
@@ -141,41 +143,44 @@
     for name in loads:
         if name not in urgent:
             loads[name].start()
+    for part, weight in enumerate((gate_h, up_h)):
+        for j in range(N_TP):
+            pltpu.make_async_copy(
+                weight.at[:, pl.ds(j * 128, 128)],
+                gateup.at[pl.ds(part * 224, 224), pl.ds((2 * (j % N_Y) + j // N_Y) * 128, 128)],
+                load_sem.at[len(loads)],
+            ).start()
     rows = expin[...].astype(F32)
     scale = lax.rsqrt(jnp.mean(rows * rows, axis=-1, keepdims=True) + EPS)
     normed_b = jnp.concatenate(
         [
             (expin[:, part].astype(F32) * scale * egain[:, part]).astype(BF16)
-            for part in (features(tp), features(across))
+            for part in (features(low), features(low + N_Y))
         ],
         axis=1,
     )
-    both_parts = nn(onehot[...], normed_b).astype(BF16)
-    send_b[0], send_b[1] = both_parts[:, :128], both_parts[:, 128:]
+    send_b[...] = nn(onehot[...], normed_b).astype(BF16)
 
     pl.semaphore_wait(barrier, N_EP - 1 + 3)
 
-    def dispatch(b, i, part):
-        dz, dx = GROUPS[b][i]
-        target = ep_at(-dz, -dx)
-        return pltpu.make_async_remote_copy(
-            src_ref=send_b.at[part, pl.ds(pl.multiple_of(target * CAP, CAP), CAP)],
-            dst_ref=xs.at[b, pl.ds(i * CAP, CAP), features((tp, across)[part])],
-            send_sem=disp_s.at[0],
-            recv_sem=disp_r.at[b],
-            device_id=(target, tp),
-            device_id_type=MESH,
-        )
+    def dispatch_parts(b, i, target):
+        rows = pl.ds(pl.multiple_of(target * CAP, CAP), CAP)
+        if COPIES[b] == 2:
+            to = pl.ds(pl.multiple_of(low * 256, 256), 256)
+            return send_b.at[rows], xs.at[b, pl.ds(i * CAP, CAP), to]
+        return send_b.at[rows, features(tp // N_Y)], xs.at[b, pl.ds(i * CAP, CAP), place(tp)]
 
     def dispatch_batch(b):
-        for i, o in enumerate(GROUPS[b]):
-            for part, chunk in enumerate((tp, across)[: COPIES[b]]):
-                if o != (0, 0):
-                    dispatch(b, i, part).start()
-                else:
-                    xs[b, i * CAP : (i + 1) * CAP, features(chunk)] = send_b[
-                        part, pl.ds(pl.multiple_of(ep * CAP, CAP), CAP), :
-                    ]
+        for i, (dz, dx) in enumerate(GROUPS[b]):
+            target = ep_at(-dz, -dx)
+            src, dst = dispatch_parts(b, i, target)
+            if (dz, dx) == (0, 0):
+                dst[...] = src[...]
+            else:
+                pltpu.make_async_remote_copy(
+                    src_ref=src, dst_ref=dst, send_sem=disp_s.at[0], recv_sem=disp_r.at[b],
+                    device_id=(target, tp), device_id_type=MESH,
+                ).start()
 
     for b in range(EARLY):
         dispatch_batch(b)
@@ -240,7 +245,7 @@
 
     def piece_of(kind, b):
         if kind == ROWS:
-            return lambda j, h=0, n=1: xs.at[b, pl.ds(h * 128, 256 // n), features(j)]
+            return lambda j, h=0, n=1: xs.at[b, pl.ds(h * 128, 256 // n), place(j)]
         if kind == HIDDEN:
             return lambda j, h=0, n=1: hs.at[b, pl.ds(pl.multiple_of(j * 224 + h * 112, 16), 224 // n)]
         return lambda j, h=0, n=1: grouped.at[pl.ds(pl.multiple_of(j * 64 + h * 32, 32), 64 // n)]
@@ -289,18 +294,18 @@
 
         def first(self):
             ref = self.piece(tp)
+            self.to_mate(ref)
             self.on_ring(ref, 1, 1)
             self.on_ring(ref, -1, 1)
-            self.to_mate(ref)
 
         def step(self, k):
             for way, h in ((1, 0), (-1, 1)):
                 j = ring_tp(-way * k)
                 ref = self.piece(j) if k < 4 else self.piece(j, h, 2)
                 arrived(ref, self.received(way, k))
+                self.to_mate(ref)
                 if k < 4:
                     self.on_ring(ref if k < 3 else self.piece(j, h, 2), way, k + 1)
-                self.to_mate(ref)
 
         def finish(self):
             arrived(self.part(N_Y), part_r.at[self.n])
@@ -312,17 +317,17 @@
         def first(self):
             for k, j in enumerate((tp, across)):
                 ref = self.piece(j)
+                self.to_mate(ref)
                 self.on_ring(ref, 1, 1 + k)
                 self.on_ring(ref, -1, 1 + k)
-                self.to_mate(ref)
 
         def step(self, k):
             for way in (1, -1):
                 ref = self.piece(ring_tp((-way, 3 * way, -2 * way)[k - 1]))
                 arrived(ref, self.received(way, k))
+                self.to_mate(ref)
                 if k == 1:
                     self.on_ring(ref, way, 3)
-                self.to_mate(ref)
 
         def all_sent(self):
             left(self.part(N_TP - 2), sent.at[self.n])
@@ -364,8 +369,7 @@
         mixed_o[...] = nt(identity, mixed_t).astype(BF16)
 
     def wait_weights():
-        loads["gate"].wait()
-        loads["up"].wait()
+        pltpu.make_async_copy(gateup, gateup, load_sem.at[len(loads)]).wait()
 
     gathers = {(MIXER, 0): Gather(2 * BATCHES, MIXER, 0)}
     for b in range(BATCHES):
@@ -404,8 +408,7 @@
     for gather in gathers.values():
         gather.all_sent()
     for b in range(BATCHES):
-        for _ in range(COPIES[b]):
-            left(send_b.at[0, pl.ds(0, remote_rows(b))], disp_s.at[0])
+        left(send_b.at[pl.ds(0, remote_rows(b)), pl.ds(0, 128 * COPIES[b])], disp_s.at[0])
     left(ret.at[pl.ds(0, others)], ret_s.at[0])
 
 
@@ -444,7 +447,7 @@
             vmem((N_EP, 256), F32),
             vmem((2, 256, 1024), BF16),
             vmem((1024, 256), BF16),
-            vmem((2, 1024, 128), BF16),
+            vmem((1024, 256), BF16),
             vmem((BATCHES, 256, 2048), BF16),
             vmem((BATCHES, 3584, 256), BF16),
             vmem((BATCHES, 256, 128), BF16),

time: 91 us -> 87.2 us (0.958)
  Pallas kernels: 88.2 us -> 84.4 us
    pallas_call x1, Pallas kernels: 88.2 us -> 84.4 us  [per_device(): pl.pallas_call(kernel, name='mixer_and_experts', out_shape=(jax.ShapeDtyp...]
where the time goes in v3:
time: 87.2 us; the launch traced here: 87 us
  Pallas kernels  84.4 us (97%)
  local copies, waits for them, and re-layouts  2.04 us (2%)
    pallas_call x1, Pallas kernels, per_device(): pl.pallas_call(kernel, name='mixer_and_experts', out_shape=(jax.ShapeDtyp...  84.4 us
    unnamed x4, local copies, waits for them, and re-layouts  2.04 us

profile of v3, /device:TPU:1, one launch (start us, length us, event | category | flops | bytes accessed | tf_op | source)
XLA Modules:
  0.0 87.0 jit_solution(2738593061667432917)
XLA Ops:
  0.6 84.4 %mixer_and_experts.1 = (bf16[128,128]{1,0:T(8,128)(2,1)}, bf16[256,128]{1,0:T(8,128)(2,1)}) custom-call(bf16[128,2048]{1,0:T(8,128)(2,1)} %mixin_h.1, f32[1,2048]{1,0:T(1,128)} %bitcast.21, bf16[64,2048]{1,0:T(8,128)(2,1)} %bitcast.18, bf16[64,2048]{1,0:T(8,128)(2,1)} %bitcast.19, bf16[64,2048]{1,0:T(8,128)(2,1)} %bitcast.20, bf16[3,64]{1,0:T(4,128)(2,1)} %conv_h.1, ...), custom_call_target="tpu_custom_call" | custom-call | tf_op jit(solution)/shard_map/mixer_and_experts/pallas_call | solution.py:423
  85.0 0.0 copy-start
  85.0 1.4 %copy.19 = bf16[128,128]{1,0:T(8,128)(2,1)} copy(bf16[128,128]{1,0:T(8,128)(2,1)} %get-tuple-element.4) | data formatting | bytes 65536
  86.4 0.0 copy-done
  86.4 0.6 copy.20
Async XLA Ops:
  85.0 1.4 %copy-start = (bf16[256,128]{1,0:T(8,128)(2,1)S(1)}, bf16[256,128]{1,0:T(8,128)(2,1)}, u32[]{:S(2)}) copy-start(bf16[256,128]{1,0:T(8,128)(2,1)} %get-tuple-element.5) | copy-start | bytes 196612

commit v4 on v3

--- a/solution.py
+++ b/solution.py
@@ -18,24 +18,24 @@
 BATCHES = 4
 EARLY = 2
 ROWS, HIDDEN, MIXER = "x", "h", "m"
-END = 9
+ACROSS, END = 5, 9
 ORDER = (
-    (ROWS, 0, 0), (ROWS, 1, 0), (ROWS, 0, 1), (ROWS, 1, 1), (ROWS, 0, 2), (ROWS, 2, 0),
-    (ROWS, 1, 2), (ROWS, 3, 0), (ROWS, 1, 3), (ROWS, 2, 1), (ROWS, 1, END), (ROWS, 0, 3),
-    (ROWS, 3, 1), (ROWS, 2, 2), (HIDDEN, 1, 0), (ROWS, 0, END), (HIDDEN, 0, 0), (ROWS, 3, 2),
-    (ROWS, 2, 3), (ROWS, 2, END), (ROWS, 3, 3), (HIDDEN, 2, 0), (ROWS, 3, END), (HIDDEN, 3, 0),
-    (HIDDEN, 1, 1), (HIDDEN, 2, 1), (HIDDEN, 3, 1), (MIXER, 0, 0), (HIDDEN, 1, 2), (HIDDEN, 3, 2),
-    (HIDDEN, 0, 1), (HIDDEN, 2, 2), (HIDDEN, 3, 3), (HIDDEN, 0, 2), (MIXER, 0, 1), (HIDDEN, 2, 3),
-    (HIDDEN, 1, 3), (HIDDEN, 3, 4), (HIDDEN, 0, 3), (HIDDEN, 3, END), (HIDDEN, 2, 4), (MIXER, 0, 2),
-    (HIDDEN, 1, 4), (HIDDEN, 2, END), (HIDDEN, 0, 4), (HIDDEN, 1, END), (MIXER, 0, 3), (HIDDEN, 0, END),
-    (MIXER, 0, 4), (MIXER, 0, END),
+    (ROWS, 0, 0), (ROWS, 0, 5), (ROWS, 1, 0), (ROWS, 0, 1), (ROWS, 1, 1), (ROWS, 0, 2),
+    (ROWS, 2, 0), (ROWS, 1, 2), (ROWS, 3, 0), (ROWS, 1, 3), (ROWS, 2, 1), (ROWS, 1, END),
+    (ROWS, 0, 3), (ROWS, 3, 1), (ROWS, 2, 2), (HIDDEN, 1, 0), (ROWS, 0, END), (HIDDEN, 0, 0),
+    (ROWS, 3, 2), (ROWS, 2, 3), (ROWS, 2, END), (ROWS, 3, 3), (HIDDEN, 2, 0), (ROWS, 3, END),
+    (HIDDEN, 3, 0), (HIDDEN, 1, 1), (HIDDEN, 2, 1), (HIDDEN, 3, 1), (MIXER, 0, 0), (HIDDEN, 1, 2),
+    (HIDDEN, 3, 2), (HIDDEN, 0, 1), (HIDDEN, 2, 2), (HIDDEN, 3, 3), (HIDDEN, 0, 2), (MIXER, 0, 1),
+    (HIDDEN, 2, 3), (HIDDEN, 1, 3), (HIDDEN, 3, 4), (HIDDEN, 0, 3), (HIDDEN, 3, END), (HIDDEN, 2, 4),
+    (MIXER, 0, 2), (HIDDEN, 1, 4), (HIDDEN, 2, END), (HIDDEN, 0, 4), (HIDDEN, 1, END), (MIXER, 0, 3),
+    (HIDDEN, 0, END), (MIXER, 0, 4), (MIXER, 0, END),
 )
 CAP = 32
 PER = N_EP // BATCHES
 
 
 GROUPS = (
-    ((1, 0), (7, 0), (0, 1), (0, 3), (1, 1), (7, 3), (0, 2), (0, 0)),
+    ((0, 2), (1, 1), (7, 3), (1, 0), (7, 0), (0, 1), (0, 3), (0, 0)),
     ((2, 0), (6, 0), (1, 3), (7, 1), (2, 1), (6, 3), (1, 2), (7, 2)),
     ((2, 2), (6, 2), (3, 0), (5, 0), (2, 3), (6, 1), (3, 1), (5, 3)),
     ((4, 0), (5, 1), (3, 3), (4, 1), (5, 2), (3, 2), (4, 3), (4, 2)),
@@ -163,26 +163,30 @@
 
     pl.semaphore_wait(barrier, N_EP - 1 + 3)
 
-    def dispatch_parts(b, i, target):
+    def dispatch_parts(b, i, target, second):
         rows = pl.ds(pl.multiple_of(target * CAP, CAP), CAP)
-        if COPIES[b] == 2:
+        if COPIES[b] == 2 and b > 0:
             to = pl.ds(pl.multiple_of(low * 256, 256), 256)
             return send_b.at[rows], xs.at[b, pl.ds(i * CAP, CAP), to]
-        return send_b.at[rows, features(tp // N_Y)], xs.at[b, pl.ds(i * CAP, CAP), place(tp)]
-
-    def dispatch_batch(b):
+        half, chunk = (1 - tp // N_Y, across) if second else (tp // N_Y, tp)
+        return send_b.at[rows, features(half)], xs.at[b, pl.ds(i * CAP, CAP), place(chunk)]
+
+    def dispatch_batch(b, second=False):
         for i, (dz, dx) in enumerate(GROUPS[b]):
             target = ep_at(-dz, -dx)
-            src, dst = dispatch_parts(b, i, target)
+            src, dst = dispatch_parts(b, i, target, second)
             if (dz, dx) == (0, 0):
                 dst[...] = src[...]
             else:
                 pltpu.make_async_remote_copy(
-                    src_ref=src, dst_ref=dst, send_sem=disp_s.at[0], recv_sem=disp_r.at[b],
+                    src_ref=src, dst_ref=dst, send_sem=disp_s.at[0],
+                    recv_sem=disp_r.at[BATCHES if second else b],
                     device_id=(target, tp), device_id_type=MESH,
                 ).start()
 
-    for b in range(EARLY):
+    dispatch_batch(0)
+    dispatch_batch(0, second=True)
+    for b in range(1, EARLY):
         dispatch_batch(b)
 
     for name in ("mixin", "mgain", "outer", "inner", "value"):
@@ -315,11 +319,15 @@
 
     class PairGather(Gather):
         def first(self):
-            for k, j in enumerate((tp, across)):
-                ref = self.piece(j)
-                self.to_mate(ref)
-                self.on_ring(ref, 1, 1 + k)
-                self.on_ring(ref, -1, 1 + k)
+            super().first()
+            if self.n > 0:
+                self.second()
+
+        def second(self):
+            ref = self.piece(across)
+            self.to_mate(ref)
+            self.on_ring(ref, 1, 2)
+            self.on_ring(ref, -1, 2)
 
         def step(self, k):
             for way in (1, -1):
@@ -333,7 +341,8 @@
             left(self.part(N_TP - 2), sent.at[self.n])
 
     def wait_dispatched(b):
-        arrived(xs.at[b, pl.ds(0, remote_rows(b)), pl.ds(0, 128 * COPIES[b])], disp_r.at[b])
+        width = 128 if b == 0 else 128 * COPIES[b]
+        arrived(xs.at[b, pl.ds(0, remote_rows(b)), pl.ds(0, width)], disp_r.at[b])
 
     def hidden(b):
         both = nt(gateup[...], xs[b])
@@ -389,6 +398,9 @@
                 prepare_combine()
             elif kind == ROWS and b == 1:
                 prepare_down()
+        elif step == ACROSS:
+            arrived(xs.at[0, pl.ds(0, remote_rows(0)), pl.ds(0, 128)], disp_r.at[BATCHES])
+            gather.second()
         elif step < END:
             gather.step(step)
         else:
@@ -460,7 +472,7 @@
             vmem((64, 128), F32),
             dma((15,)),
             dma((1,)),
-            dma((BATCHES,)),
+            dma((BATCHES + 1,)),
             dma((1,)),
             dma((1,)),
             dma((phases,)),

time: 87.2 us -> 87 us (level)
  no operation moved by 1% of the time
where the time goes in v4:
time: 87 us; the launch traced here: 86.8 us
  Pallas kernels  84.1 us (97%)
  local copies, waits for them, and re-layouts  2.04 us (2%)
    pallas_call x1, Pallas kernels, per_device(): pl.pallas_call(kernel, name='mixer_and_experts', out_shape=(jax.ShapeDtyp...  84.1 us
    unnamed x4, local copies, waits for them, and re-layouts  2.04 us

profile of v4, /device:TPU:1, one launch (start us, length us, event | category | flops | bytes accessed | tf_op | source)
XLA Modules:
  0.0 86.8 jit_solution(620707475423783713)
XLA Ops:
  0.6 84.1 %mixer_and_experts.1 = (bf16[128,128]{1,0:T(8,128)(2,1)}, bf16[256,128]{1,0:T(8,128)(2,1)}) custom-call(bf16[128,2048]{1,0:T(8,128)(2,1)} %mixin_h.1, f32[1,2048]{1,0:T(1,128)} %bitcast.21, bf16[64,2048]{1,0:T(8,128)(2,1)} %bitcast.18, bf16[64,2048]{1,0:T(8,128)(2,1)} %bitcast.19, bf16[64,2048]{1,0:T(8,128)(2,1)} %bitcast.20, bf16[3,64]{1,0:T(4,128)(2,1)} %conv_h.1, ...), custom_call_target="tpu_custom_call" | custom-call | tf_op jit(solution)/shard_map/mixer_and_experts/pallas_call | solution.py:435
  84.8 0.0 copy-start
  84.8 1.4 %copy.19 = bf16[128,128]{1,0:T(8,128)(2,1)} copy(bf16[128,128]{1,0:T(8,128)(2,1)} %get-tuple-element.4) | data formatting | bytes 65536
  86.2 0.0 copy-done
  86.2 0.6 copy.20
Async XLA Ops:
  84.8 1.4 %copy-start = (bf16[256,128]{1,0:T(8,128)(2,1)S(1)}, bf16[256,128]{1,0:T(8,128)(2,1)}, u32[]{:S(2)}) copy-start(bf16[256,128]{1,0:T(8,128)(2,1)} %get-tuple-element.5) | copy-start | bytes 196612
